TPU v7x, 32 devices: a whole 2x2x4 slice. The times are simulated.
32 devices in a mesh: ep: 4 (over y, x), tp: 8 (over z, core).
Axes of the slice: x: 2, y: 2, z: 4, core: 2. Of those that a mesh axis runs over, the one named last changes fastest.
Arguments:
- pool_input: bfloat16 [4096, 1024], P('ep', 'tp'), may hold values from -6 to 6
- pool_gain: float32 [1024], P('tp'), may hold values from 0.1 to 1.9
- mix_weight: bfloat16 [1024, 2048], P('tp'), may hold values from -0.1875 to 0.1875
- moe_input: bfloat16 [8192, 2048], P(('ep', 'tp')), may hold values from -6 to 6
- moe_gain: float32 [2048], replicated, may hold values from 0.1 to 1.9
- expert_ids: int32 [8192, 2], P(('ep', 'tp')), may hold values from 0 to 15, as said below
- route_weight: float32 [8192, 2], P(('ep', 'tp')), may hold values from 0.2 to 1
- gate_weight: bfloat16 [16, 2048, 1024], P('ep', None, 'tp'), may hold values from -0.125 to 0.125
- up_weight: bfloat16 [16, 2048, 1024], P('ep', None, 'tp'), may hold values from -0.125 to 0.125
- down_weight: bfloat16 [16, 2048, 1024], P('ep', None, 'tp'), may hold values from -0.1875 to 0.1875
Outputs:
- mixed_out: bfloat16 [4096, 2048], P(('ep', 'tp'))
- moe_out: bfloat16 [8192, 2048], P(('ep', 'tp'))
Inputs may be any that keep to these rules, and one draw needn't show every extreme that they name: `expert_ids`: each row names 2 different experts of one group of 4 consecutive experts. In each aligned block of 256 rows (the rows of one device) no expert is named by more than 48 rows, and some expert is named by exactly 48 rows.
All inputs are finite; a program needn't handle non-finite values.
Results may differ from a plain program's by a relative error of at most 0.012.
Values may be sent and summed in bfloat16 or wider, within the bound.
A program may use at most 128 MiB of HBM per device.

v0:
```python
import jax
import jax.numpy as jnp
from jax import lax
from jax.sharding import PartitionSpec as P

GROUP_CH = 256
EXPERTS = 16
TOP = 2
CAP = 48
eps_norm = 1e-06


def from_behind(shard, axis, by):
    peers = lax.axis_size(axis)
    pairs = [(i, i + by) for i in range(peers) if 0 <= i + by < peers]
    return lax.ppermute(shard, axis, pairs)


def window_sums(extended, row_count):
    level_sum = extended
    stride = 1
    outputs = []
    for doubling in range(4):
        level_sum = level_sum[stride:] + level_sum[:-stride]
        stride = stride * 2
        outputs.append(level_sum[level_sum.shape[0] - row_count :])
    return outputs


def pool_mixer(pool_input, pool_gain):
    row_count, channels = pool_input.shape
    carried = from_behind(pool_input[row_count - 15 :], "ep", 1)
    extended = jnp.concatenate([carried, pool_input], axis=0).astype(jnp.float32)
    window_list = window_sums(extended, row_count)
    channel_ids = lax.axis_index("tp") * channels + lax.iota(jnp.int32, channels)
    group_ids = channel_ids // GROUP_CH
    position = lax.axis_index("ep") * row_count + lax.iota(jnp.int32, row_count)
    summed = jnp.zeros((row_count, channels), jnp.float32)
    widths = jnp.zeros((channels,), jnp.int32)
    for index_group in range(4):
        inside = group_ids == index_group
        summed = jnp.where(inside[None, :], window_list[index_group], summed)
        widths = jnp.where(inside, 2 ** (index_group + 1), widths)
    counted = jnp.minimum(position[:, None] + 1, widths[None, :]).astype(jnp.float32)
    values = extended[15:]
    return ((summed / counted - values) * pool_gain).astype(jnp.bfloat16)


def route_slots(expert_ids):
    flat_ids = expert_ids.reshape(-1)
    marked = (flat_ids[:, None] == lax.iota(jnp.int32, EXPERTS)[None, :]).astype(jnp.int32)
    before_count = jnp.cumsum(marked, axis=0) - marked
    ranked = jnp.sum(before_count * marked, axis=1)
    return (flat_ids * CAP + ranked).reshape(expert_ids.shape)


def body(
    pool_input,
    pool_gain,
    mix_weight,
    moe_input,
    moe_gain,
    expert_ids,
    route_weight,
    gate_weight,
    up_weight,
    down_weight,
):
    pooled = pool_mixer(pool_input, pool_gain)
    regrouped = lax.all_to_all(pooled, "tp", split_axis=0, concat_axis=1, tiled=True)
    mixed_sum = jnp.dot(
        regrouped,
        lax.all_gather(mix_weight, "tp", axis=0, tiled=True),
        preferred_element_type=jnp.float32,
    )
    mixed_out = mixed_sum.astype(jnp.bfloat16)
    inputs = moe_input.astype(jnp.float32)
    scale_rows = lax.rsqrt(jnp.mean(inputs * inputs, axis=-1, keepdims=True) + eps_norm)
    normed = (inputs * scale_rows * moe_gain).astype(jnp.bfloat16)
    slots = route_slots(expert_ids)
    slot_index = lax.iota(jnp.int32, EXPERTS * CAP)
    placing = (
        (slot_index[:, None] == slots[None, :, 0]) | (slot_index[:, None] == slots[None, :, 1])
    ).astype(jnp.bfloat16)
    outgoing = jnp.dot(placing, normed, preferred_element_type=jnp.float32).astype(jnp.bfloat16)
    outgoing = outgoing.reshape(EXPERTS, CAP, normed.shape[1])
    arrived = lax.all_to_all(outgoing, "ep", split_axis=0, concat_axis=1, tiled=True)
    gate_piece = lax.all_gather(gate_weight, "tp", axis=2, tiled=True)
    up_piece = lax.all_gather(up_weight, "tp", axis=2, tiled=True)
    down_piece = lax.all_gather(down_weight, "tp", axis=2, tiled=True)
    gate_part = jnp.einsum("erd,edf->erf", arrived, gate_piece, preferred_element_type=jnp.float32)
    upward = jnp.einsum("erd,edf->erf", arrived, up_piece, preferred_element_type=jnp.float32)
    hidden = (jax.nn.silu(gate_part) * upward).astype(jnp.bfloat16)
    expert_sum = jnp.einsum("erf,edf->erd", hidden, down_piece, preferred_element_type=jnp.float32)
    expert_rows = expert_sum.astype(jnp.bfloat16)
    returned = lax.all_to_all(expert_rows, "ep", split_axis=1, concat_axis=0, tiled=True)
    returned_rows = returned.reshape(EXPERTS * CAP, returned.shape[2])
    combined = jnp.zeros((normed.shape[0], normed.shape[1]), jnp.float32)
    for route_index in range(TOP):
        picking = (slots[:, route_index][:, None] == slot_index[None, :]).astype(jnp.bfloat16)
        chosen_rows = jnp.dot(picking, returned_rows, preferred_element_type=jnp.float32)
        combined = combined + route_weight[:, route_index : route_index + 1] * chosen_rows
    moe_out = combined.astype(jnp.bfloat16)
    return (mixed_out, moe_out)


def solution(mesh):
    return jax.shard_map(
        body,
        mesh=mesh,
        in_specs=(
            P("ep", "tp"),
            P("tp"),
            P("tp", None),
            P(("ep", "tp"), None),
            P(),
            P(("ep", "tp"), None),
            P(("ep", "tp"), None),
            P("ep", None, "tp"),
            P("ep", None, "tp"),
            P("ep", None, "tp"),
        ),
        out_specs=(P(("ep", "tp"), None), P(("ep", "tp"), None)),
        check_vma=False,
    )
```

profile of v0, /device:TPU:0, one launch (start us, length us, event | category | flops | bytes accessed | tf_op | source)
XLA Modules:
  0.0 554.3 jit_solution(15557223583954882724)
XLA Ops:
  7.2 0.0 copy-start.5
  7.2 0.0 copy-start.1
  7.2 0.0 all-gather.7.cloned.1.call-start
  7.2 0.7 all-gather.7.cloned.1.call-update
  7.9 0.0 copy-start.4
  7.9 0.0 all-gather.11.cloned.1.call-start
  8.0 0.7 all-gather.11.cloned.1.call-update
  8.7 0.0 all-gather.9.cloned.1.call-start
  8.7 0.7 all-gather.9.cloned.1.call-update
  9.4 0.0 copy-done.5
  9.4 0.1 copy.47
  9.6 0.1 eq.138
  9.7 0.1 eq.134
  9.9 1.2 reduce-window.6
  11.0 0.2 slice_reduce_fusion
  11.3 0.1 fusion.23
  11.4 0.1 reduce_sum.21
  11.5 0.1 copy.50
  11.6 0.0 copy-done.1
  11.6 0.3 fusion.2
  11.9 0.0 copy-done.4
  12.0 2.8 convolution_convert_fusion
  14.7 0.0 copy-start.3
  14.7 5.3 all-to-all-start.1
  20.0 0.0 copy-start.7
  20.0 0.0 all-gather.5.cloned.1.call-start
  20.1 0.0 copy-done.3
  20.1 3.9 collective-permute-start
  24.0 0.0 all-gather.5.cloned.1.call-update
  24.1 30.0 %collective-permute-done = bf16[15,128]{1,0:T(8,128)(2,1)S(1)} collective-permute-done((bf16[15,128]{1,0:T(8,128)(2,1)S(1)}, bf16[15,128]{1,0:T(8,128)(2,1)S(1)}, u32[]{:S(2)}, u32[]{:S(2)}) %collective-permute-start) | collective-permute-done | bytes 3872 | tf_op jit(solution)/shard_map/ppermute | solution.py:16
  54.1 0.1 maximum_convert_fusion
  54.2 0.1 slice_add_fusion.1
  54.2 0.1 slice_add_fusion
  54.3 0.1 slice_add_fusion.2
  54.3 0.0 copy-done.7
  54.4 1.1 fusion.12
  55.4 0.8 all-to-all-done.1
  56.2 5.2 all-to-all-start
  61.4 1.9 copy.51
  63.3 107.9 %all-gather.7.cloned.1.call-done = bf16[4,2048,1024]{2,1,0:T(8,128)(2,1)} async-done(((bf16[4,2048,128]{2,1,0:T(8,128)(2,1)}), bf16[4,2048,1024]{2,1,0:T(8,128)(2,1)}) %all-gather.7.cloned.1.call-update) | async-done | bytes 16777232 | tf_op jit(solution)/shard_map/all_gather | solution.py:88
  171.2 0.0 copy-start
  171.2 11.9 %fusion.28 = f32[4,192,1024]{2,1,0:T(8,128)} fusion(bf16[4,192,2048]{2,1,0:T(8,128)(2,1)} %bitcast.48, bf16[4,2048,1024]{2,1,0:T(8,128)(2,1)} %all-gather.7.cloned.1.call-done), kind=kOutput, calls=%fused_computation.62 | convolution fusion | flops 3221225472 | bytes 23068672 | tf_op jit(solution)/shard_map/erd,edf->erf/dot_general | solution.py:91
  183.2 142.6 %all-gather.11.cloned.1.call-done = bf16[4,2048,1024]{2,1,0:T(8,128)(2,1)} async-done(((bf16[4,2048,128]{2,1,0:T(8,128)(2,1)}), bf16[4,2048,1024]{2,1,0:T(8,128)(2,1)}) %all-gather.11.cloned.1.call-update) | async-done | bytes 16777232 | tf_op jit(solution)/shard_map/all_gather | solution.py:90
  325.8 151.6 %all-gather.9.cloned.1.call-done = bf16[4,2048,1024]{2,1,0:T(8,128)(2,1)} async-done(((bf16[4,2048,128]{2,1,0:T(8,128)(2,1)}), bf16[4,2048,1024]{2,1,0:T(8,128)(2,1)}) %all-gather.9.cloned.1.call-update) | async-done | bytes 16777232 | tf_op jit(solution)/shard_map/all_gather | solution.py:89
  477.4 0.0 copy-done
  477.4 17.7 %convolution_convert_fusion.1 = bf16[4,192,2048]{2,1,0:T(8,128)(2,1)} fusion(bf16[4,2048,1024]{2,1,0:T(8,128)(2,1)} %all-gather.11.cloned.1.call-done, f32[4,192,1024]{2,1,0:T(8,128)} %fusion.28, bf16[4,192,2048]{2,1,0:T(8,128)(2,1)S(1)} %bitcast.49, bf16[4,2048,1024]{2,1,0:T(8,128)(2,1)} %all-gather.9.cloned.1.call-done), kind=kOutput, calls=%fused_computation.1 | convolution fusion | flops 6448742400 | bytes 42991616 | tf_op jit(solution)/shard_map/erf,edf->erd/dot_general | solution.py:94
  495.1 6.0 %copy.52 = bf16[4,192,2048]{2,0,1:T(4,128)(2,1)} copy(bf16[4,192,2048]{2,1,0:T(8,128)(2,1)} %convolution_convert_fusion.1) | data formatting | bytes 6291456 | tf_op jit(solution)/shard_map/convert_element_type | solution.py:95
  501.1 0.0 copy-start.6
  501.1 0.0 all-to-all-done
  501.1 0.0 copy-start.2
  501.1 0.7 copy-done.2
  501.8 3.9 all-to-all-start.2
  505.7 0.0 copy-done.6
  505.7 1.1 copy.46
  506.9 17.0 %all-gather.5.cloned.1.call-done = bf16[1024,2048]{1,0:T(8,128)(2,1)} async-done(((bf16[128,2048]{1,0:T(8,128)(2,1)}), bf16[1024,2048]{1,0:T(8,128)(2,1)}) %all-gather.5.cloned.1.call-update) | async-done | bytes 4194320 | tf_op jit(solution)/shard_map/all_gather | solution.py:73
  523.9 3.7 convolution_convert_fusion.2
  527.6 14.8 %all-to-all-done.2 = bf16[4,192,2048]{2,0,1:T(4,128)(2,1)S(1)} async-done(((bf16[4,192,2048]{2,0,1:T(4,128)(2,1)}), bf16[4,192,2048]{2,0,1:T(4,128)(2,1)S(1)}, u32[]{:S(2)}, u32[]{:S(2)}) %all-to-all-start.2) | async-done | bytes 3145760 | tf_op jit(solution)/shard_map/all_to_all | solution.py:96
  542.5 1.7 copy.53
  544.2 0.4 copy.54
  544.6 1.0 convolution_multiply_fusion.1
  545.7 2.1 fusion.1
  (12 shorter events, 0.1 us)
Async XLA Ops:
  7.2 2.3 copy-start.5
  7.2 4.4 copy-start.1
  7.2 164.1 %all-gather.7.cloned.1.call-start = ((), (), s32[]{:S(2)}) async-start(), calls=%async_computation.4 | async-start | bytes 18874368 | tf_op jit(solution)/shard_map/all_gather | solution.py:88
  7.9 4.0 copy-start.4
  7.9 317.8 %all-gather.11.cloned.1.call-start = ((), (), s32[]{:S(2)}) async-start(), calls=%async_computation.6 | async-start | bytes 18874368 | tf_op jit(solution)/shard_map/all_gather | solution.py:90
  8.7 468.7 %all-gather.9.cloned.1.call-start = ((), (), s32[]{:S(2)}) async-start(), calls=%async_computation.5 | async-start | bytes 18874368 | tf_op jit(solution)/shard_map/all_gather | solution.py:89
  14.7 5.3 copy-start.3
  14.7 41.5 %all-to-all-start.1 = ((bf16[16,48,2048]{2,1,0:T(8,128)(2,1)}), bf16[16,48,2048]{2,1,0:T(8,128)(2,1)S(1)}, u32[]{:S(2)}, u32[]{:S(2)}) async-start(bf16[16,48,2048]{2,1,0:T(8,128)(2,1)} %bitcast.7), calls=%async_computation.1 | async-start | bytes 6291456 | tf_op jit(solution)/shard_map/all_to_all | solution.py:87
  20.0 34.3 %copy-start.7 = (f32[128]{0:T(128)S(1)}, f32[128]{0:T(128)}, u32[]{:S(2)}) copy-start(f32[128]{0:T(128)} %param.11) | copy-start | bytes 1540
  20.0 503.9 %all-gather.5.cloned.1.call-start = ((), (), s32[]{:S(2)}) async-start(), calls=%async_computation.3 | async-start | bytes 4718592 | tf_op jit(solution)/shard_map/all_gather | solution.py:73
  20.1 34.0 %collective-permute-start = (bf16[15,128]{1,0:T(8,128)(2,1)S(1)}, bf16[15,128]{1,0:T(8,128)(2,1)S(1)}, u32[]{:S(2)}, u32[]{:S(2)}) collective-permute-start(bf16[15,128]{1,0:T(8,128)(2,1)S(1)} %slice.57), channel_id=1, source_target_pairs={{0,8},{8,16},{16,24},{1,9},{9,17},{17,25},{2,10},{10,18},{18,26},{... | collective-permute-start | bytes 11528 | tf_op jit(solution)/shard_map/ppermute | solution.py:16
  56.2 444.9 %all-to-all-start = ((bf16[8,128,128]{2,1,0:T(8,128)(2,1)}), bf16[8,128,128]{2,1,0:T(8,128)(2,1)S(1)}, u32[]{:S(2)}, u32[]{:S(2)}) async-start(bf16[8,128,128]{2,1,0:T(8,128)(2,1)} %bitcast), calls=%async_computation | async-start | bytes 524288 | tf_op jit(solution)/shard_map/all_to_all | solution.py:70
  171.2 306.1 %copy-start = (bf16[4,4,48,2048]{3,2,0,1:T(8,128)(2,1)S(1)}, bf16[4,4,48,2048]{3,2,0,1:T(8,128)(2,1)}, u32[]{:S(2)}) copy-start(bf16[4,4,48,2048]{3,2,0,1:T(8,128)(2,1)} %copy.51) | copy-start | bytes 9437188
  501.1 4.6 copy-start.6
  501.1 0.7 copy-start.2
  501.8 40.6 %all-to-all-start.2 = ((bf16[4,192,2048]{2,0,1:T(4,128)(2,1)}), bf16[4,192,2048]{2,0,1:T(4,128)(2,1)S(1)}, u32[]{:S(2)}, u32[]{:S(2)}) async-start(bf16[4,192,2048]{2,0,1:T(4,128)(2,1)} %copy.52), calls=%async_computation.2 | async-start | bytes 6291456 | tf_op jit(solution)/shard_map/all_to_all | solution.py:96
Sparse Core Ops, SparseCore 0:
  9.6 161.6 all-gather.6
  172.8 152.8 all-gather.10
  327.4 149.9 all-gather.8
  478.8 45.0 all-gather.4
where the time goes:
time: 555 us; the launch traced here: 554 us
  waiting for transfers between devices  467 us (84%)
  matrix products  39.2 us (7%)
  starting transfers between devices  18.4 us (3%)
  between operations  14 us (3%)
  local copies, waits for them, and re-layouts  12.8 us (2%)
    all_gather x1, waiting for transfers between devices, body(): up_piece = lax.all_gather(up_weight, 'tp', axis=2, tiled=True)  152 us
    all_gather x1, waiting for transfers between devices, body(): down_piece = lax.all_gather(down_weight, 'tp', axis=2, tiled=True)  143 us
    all_gather x1, waiting for transfers between devices, body(): gate_piece = lax.all_gather(gate_weight, 'tp', axis=2, tiled=True)  108 us
    ppermute x1, waiting for transfers between devices, from_behind(): return lax.ppermute(shard, axis, pairs)  30 us
    dot_general x1, matrix products, body(): jnp.einsum('erf,edf->erd', hidden, down_piece, preferred_element_type=jnp...  17.7 us
    all_gather x1, waiting for transfers between devices, body(): lax.all_gather(mix_weight, 'tp', axis=0, tiled=True)  17 us
    all_to_all x1, waiting for transfers between devices, body(): lax.all_to_all(expert_rows, 'ep', split_axis=1, concat_axis=0, tiled=True)  14.8 us
    dot_general x1, matrix products, body(): jnp.einsum('erd,edf->erf', arrived, gate_piece, preferred_element_type=jn...  11.9 us
  transfers between devices with their start and end apart: 8, of which 7 were waited for; matrix products, arithmetic and copies ran while one was open for 9% of the time, Pallas kernels for 0%

commit v1 on v0

--- a/solution.py
+++ b/solution.py
@@ -85,10 +85,21 @@
     outgoing = jnp.dot(placing, normed, preferred_element_type=jnp.float32).astype(jnp.bfloat16)
     outgoing = outgoing.reshape(EXPERTS, CAP, normed.shape[1])
     arrived = lax.all_to_all(outgoing, "ep", split_axis=0, concat_axis=1, tiled=True)
-    gate_piece = lax.all_gather(gate_weight, "tp", axis=2, tiled=True)
     up_piece = lax.all_gather(up_weight, "tp", axis=2, tiled=True)
     down_piece = lax.all_gather(down_weight, "tp", axis=2, tiled=True)
-    gate_part = jnp.einsum("erd,edf->erf", arrived, gate_piece, preferred_element_type=jnp.float32)
+    x = gate_weight
+    ways, here, step = (lax.axis_size("tp"), lax.axis_index("tp"), x.shape[2])
+    results = []
+    for far in range(ways):
+        arriving = (
+            lax.ppermute(x, "tp", [(d, (d + 1) % ways) for d in range(ways)])
+            if far + 1 < ways
+            else x
+        )
+        results.append(jnp.einsum("erd,edf->erf", arrived, x, preferred_element_type=jnp.float32))
+        x = arriving
+    line = jnp.concatenate(results[::-1], axis=2)
+    gate_part = jnp.roll(line, (here + 1) * results[0].shape[2], axis=2)
     upward = jnp.einsum("erd,edf->erf", arrived, up_piece, preferred_element_type=jnp.float32)
     hidden = (jax.nn.silu(gate_part) * upward).astype(jnp.bfloat16)
     expert_sum = jnp.einsum("erf,edf->erd", hidden, down_piece, preferred_element_type=jnp.float32)

time: 555 us -> 582 us (1.049)
  the two profiles are of different devices: /device:TPU:0 before, /device:TPU:16 now
where the time goes in v1:
time: 582 us; the launch traced here: 581 us
  waiting for transfers between devices  450 us (77%)
  matrix products  46.2 us (8%)
  starting transfers between devices  42.8 us (7%)
  local copies, waits for them, and re-layouts  24.9 us (4%)
  between operations  14 us (2%)
    ppermute x7, waiting for transfers between devices, body(): lax.ppermute(x, 'tp', [(d, (d + 1) % ways) for d in range(ways)])  433 us
    ppermute x7, starting transfers between devices, body(): lax.ppermute(x, 'tp', [(d, (d + 1) % ways) for d in range(ways)])  26.7 us
    dot_general x8, matrix products, body(): jnp.einsum('erd,edf->erf', arrived, x, preferred_element_type=jnp.float32)  19.2 us
    dot_general x1, matrix products, body(): jnp.einsum('erf,edf->erd', hidden, down_piece, preferred_element_type=jnp...  17.3 us
    all_to_all x1, waiting for transfers between devices, body(): lax.all_to_all(expert_rows, 'ep', split_axis=1, concat_axis=0, tiled=True)  15.8 us
    unnamed x44, local copies, waits for them, and re-layouts  12.1 us
  transfers between devices with their start and end apart: 14, of which 8 were waited for; matrix products, arithmetic and copies ran while one was open for 11% of the time, Pallas kernels for 0%

profile of v1, /device:TPU:16, one launch (start us, length us, event | category | flops | bytes accessed | tf_op | source)
XLA Modules:
  0.0 581.0 jit_solution(3101445564384831360)
XLA Ops:
  7.3 0.7 all-gather.6.cloned.1.call-update
  8.0 0.7 all-gather.8.cloned.1.call-update
  8.7 0.1 copy-done.1
  8.8 70.4 %collective-permute-done.1 = bf16[4,2048,128]{2,1,0:T(8,128)(2,1)S(1)} collective-permute-done((bf16[4,2048,128]{2,1,0:T(8,128)(2,1)S(1)}, bf16[4,2048,128]{2,1,0:T(8,128)(2,1)S(1)}, u32[]{:S(2)}, u32[]{:S(2)}) %collective-permute-start.1) | collective-permute-done | bytes 2097184 | tf_op jit(solution)/shard_map/ppermute | solution.py:95
  79.2 1.3 copy-done.3
  80.5 1.5 collective-permute-start.2
  82.0 68.9 %collective-permute-done.2 = bf16[4,2048,128]{2,1,0:T(8,128)(2,1)S(1)} collective-permute-done((bf16[4,2048,128]{2,1,0:T(8,128)(2,1)S(1)}, bf16[4,2048,128]{2,1,0:T(8,128)(2,1)S(1)}, u32[]{:S(2)}, u32[]{:S(2)}) %collective-permute-start.2) | collective-permute-done | bytes 2097184 | tf_op jit(solution)/shard_map/ppermute | solution.py:95
  150.9 1.4 copy-done.5
  152.3 18.6 %collective-permute-start.3 = (bf16[4,2048,128]{2,1,0:T(8,128)(2,1)S(1)}, bf16[4,2048,128]{2,1,0:T(8,128)(2,1)S(1)}, u32[]{:S(2)}, u32[]{:S(2)}) collective-permute-start(bf16[4,2048,128]{2,1,0:T(8,128)(2,1)S(1)} %collective-permute-done.2), channel_id=1, source_target_pairs={{0,1},{1,2},{2,3},{3,4},{4,5},{5,6},{6,7},{7,0},{8,9},{9,10},{10,1... | collective-permute-start | bytes 6291464 | tf_op jit(solution)/shard_map/ppermute | solution.py:95
  170.9 49.2 %collective-permute-done.3 = bf16[4,2048,128]{2,1,0:T(8,128)(2,1)S(1)} collective-permute-done((bf16[4,2048,128]{2,1,0:T(8,128)(2,1)S(1)}, bf16[4,2048,128]{2,1,0:T(8,128)(2,1)S(1)}, u32[]{:S(2)}, u32[]{:S(2)}) %collective-permute-start.3) | collective-permute-done | bytes 2097184 | tf_op jit(solution)/shard_map/ppermute | solution.py:95
  220.0 1.4 copy-done.7
  221.4 70.4 %collective-permute-done.4 = bf16[4,2048,128]{2,1,0:T(8,128)(2,1)S(1)} collective-permute-done((bf16[4,2048,128]{2,1,0:T(8,128)(2,1)S(1)}, bf16[4,2048,128]{2,1,0:T(8,128)(2,1)S(1)}, u32[]{:S(2)}, u32[]{:S(2)}) %collective-permute-start.4) | collective-permute-done | bytes 2097184 | tf_op jit(solution)/shard_map/ppermute | solution.py:95
  291.8 1.3 copy-done.9
  293.1 71.4 %collective-permute-done.5 = bf16[4,2048,128]{2,1,0:T(8,128)(2,1)} collective-permute-done((bf16[4,2048,128]{2,1,0:T(8,128)(2,1)S(1)}, bf16[4,2048,128]{2,1,0:T(8,128)(2,1)}, u32[]{:S(2)}, u32[]{:S(2)}) %collective-permute-start.5) | collective-permute-done | bytes 2097184 | tf_op jit(solution)/shard_map/ppermute | solution.py:95
  364.5 6.6 %collective-permute-start.6 = (bf16[4,2048,128]{2,1,0:T(8,128)(2,1)}, bf16[4,2048,128]{2,1,0:T(8,128)(2,1)}, u32[]{:S(2)}, u32[]{:S(2)}) collective-permute-start(bf16[4,2048,128]{2,1,0:T(8,128)(2,1)} %collective-permute-done.5), channel_id=1, source_target_pairs={{0,1},{1,2},{2,3},{3,4},{4,5},{5,6},{6,7},{7,0},{8,9},{9,10},{10,1... | collective-permute-start | bytes 6291464 | tf_op jit(solution)/shard_map/ppermute | solution.py:95
  371.1 0.1 copy.47
  371.3 0.1 eq.141
  371.4 0.1 eq.137
  371.6 1.2 reduce-window.6
  372.7 0.2 slice_reduce_fusion
  373.0 0.1 fusion.23
  373.1 0.1 reduce_sum.21
  373.2 0.1 copy.50
  373.3 0.3 fusion.2
  373.7 2.8 convolution_convert_fusion
  376.5 3.8 all-to-all-start.1
  380.3 0.0 all-gather.4.cloned.1.call-start
  380.4 3.8 collective-permute-start
  384.3 46.8 %collective-permute-done.6 = bf16[4,2048,128]{2,1,0:T(8,128)(2,1)} collective-permute-done((bf16[4,2048,128]{2,1,0:T(8,128)(2,1)}, bf16[4,2048,128]{2,1,0:T(8,128)(2,1)}, u32[]{:S(2)}, u32[]{:S(2)}) %collective-permute-start.6) | collective-permute-done | bytes 2097184 | tf_op jit(solution)/shard_map/ppermute | solution.py:95
  431.1 0.1 maximum_convert_fusion
  431.2 0.1 slice_add_fusion.1
  431.3 0.1 slice_add_fusion
  431.3 0.1 slice_add_fusion.2
  431.4 1.1 fusion.12
  432.5 4.5 all-to-all-start
  437.0 2.1 copy.51
  439.1 55.7 %collective-permute-done.7 = bf16[4,2048,128]{2,1,0:T(8,128)(2,1)} collective-permute-done((bf16[4,2048,128]{2,1,0:T(8,128)(2,1)}, bf16[4,2048,128]{2,1,0:T(8,128)(2,1)}, u32[]{:S(2)}, u32[]{:S(2)}) %collective-permute-start.7) | collective-permute-done | bytes 2097184 | tf_op jit(solution)/shard_map/ppermute | solution.py:95
  494.8 3.3 constant_dynamic-update-slice_fusion.15
  498.1 3.3 constant_dynamic-update-slice_fusion.14
  501.5 3.5 constant_dynamic-update-slice_fusion.13
  505.0 1.8 constant_dynamic-update-slice_fusion.12
  506.8 1.8 constant_dynamic-update-slice_fusion.11
  508.6 1.8 constant_dynamic-update-slice_fusion.10
  510.4 1.9 constant_dynamic-update-slice_fusion.9
  512.3 1.8 constant_dynamic-update-slice_fusion.8
  514.1 0.8 constant_dynamic-update-slice_fusion.7
  514.9 0.9 constant_dynamic-update-slice_fusion.6
  515.8 0.8 constant_dynamic-update-slice_fusion.5
  516.6 0.8 constant_dynamic-update-slice_fusion.4
  517.4 0.8 constant_dynamic-update-slice_fusion.3
  518.3 0.8 constant_dynamic-update-slice_fusion.2
  519.1 0.8 constant_dynamic-update-slice_fusion.1
  519.8 0.8 constant_dynamic-update-slice_fusion
  520.6 17.3 %convolution_convert_fusion.1 = bf16[4,192,2048]{2,1,0:T(8,128)(2,1)} fusion(bf16[4,2048,1024]{2,1,0:T(8,128)(2,1)} %all-gather.8.cloned.1.call-done, f32[4,192,2048]{2,1,0:T(8,128)} %constant_dynamic-update-slice_fusion, s32[]{:T(128)S(6)} %select_n.86, bf16[4,192,2048]{2,1,0:T(8,128)(2,1)S(1)} %bitcast.66, ...), kind=kOutput, calls=%fused_computation.1 | convolution fusion | flops 6448742400 | bytes 42991620 | tf_op jit(solution)/shard_map/erf,edf->erd/dot_general | solution.py:105
  538.0 5.9 %copy.52 = bf16[4,192,2048]{2,0,1:T(4,128)(2,1)} copy(bf16[4,192,2048]{2,1,0:T(8,128)(2,1)} %convolution_convert_fusion.1) | data formatting | bytes 6291456 | tf_op jit(solution)/shard_map/convert_element_type | solution.py:106
  543.9 0.7 copy-done.12
  544.6 3.9 all-to-all-start.2
  548.5 1.1 copy.46
  549.7 3.7 convolution_convert_fusion.2
  553.4 15.8 %all-to-all-done.2 = bf16[4,192,2048]{2,0,1:T(4,128)(2,1)S(1)} async-done(((bf16[4,192,2048]{2,0,1:T(4,128)(2,1)}), bf16[4,192,2048]{2,0,1:T(4,128)(2,1)S(1)}, u32[]{:S(2)}, u32[]{:S(2)}) %all-to-all-start.2) | async-done | bytes 3145760 | tf_op jit(solution)/shard_map/all_to_all | solution.py:107
  569.2 1.7 copy.53
  570.9 0.4 copy.54
  571.3 1.0 convolution_multiply_fusion.1
  572.4 2.1 fusion.1
  (55 shorter events, 0.3 us)
Async XLA Ops:
  7.2 1.6 copy-start.1
  7.2 364.0 %copy-start.15 = (s32[256,2]{0,1:T(2,128)S(1)}, s32[256,2]{0,1:T(2,128)}, u32[]{:S(2)}) copy-start(s32[256,2]{0,1:T(2,128)} %param.15) | copy-start | bytes 6148
  7.2 366.1 %copy-start.11 = (bf16[256,2048]{1,0:T(8,128)(2,1)S(1)}, bf16[256,2048]{1,0:T(8,128)(2,1)}, u32[]{:S(2)}) copy-start(bf16[256,2048]{1,0:T(8,128)(2,1)} %param.13) | copy-start | bytes 3145732
  7.2 366.5 %copy-start.14 = (f32[2048]{0:T(1024)S(1)}, f32[2048]{0:T(1024)}, u32[]{:S(2)}) copy-start(f32[2048]{0:T(1024)} %param.14) | copy-start | bytes 24580
  7.2 513.4 %all-gather.6.cloned.1.call-start = ((), (), s32[]{:S(2)}) async-start(), calls=%async_computation.4 | async-start | bytes 18874368 | tf_op jit(solution)/shard_map/all_gather | solution.py:88
  7.9 512.7 %all-gather.8.cloned.1.call-start = ((), (), s32[]{:S(2)}) async-start(), calls=%async_computation.5 | async-start | bytes 18874368 | tf_op jit(solution)/shard_map/all_gather | solution.py:89
  8.8 70.4 %collective-permute-start.1 = (bf16[4,2048,128]{2,1,0:T(8,128)(2,1)S(1)}, bf16[4,2048,128]{2,1,0:T(8,128)(2,1)S(1)}, u32[]{:S(2)}, u32[]{:S(2)}) collective-permute-start(bf16[4,2048,128]{2,1,0:T(8,128)(2,1)S(1)} %copy-done.1), channel_id=1, source_target_pairs={{0,1},{1,2},{2,3},{3,4},{4,5},{5,6},{6,7},{7,0},{8,9},{9,10},{10,1... | collective-permute-start | bytes 6291464 | tf_op jit(solution)/shard_map/ppermute | solution.py:95
  79.2 1.3 copy-start.3
  80.5 70.4 %collective-permute-start.2 = (bf16[4,2048,128]{2,1,0:T(8,128)(2,1)S(1)}, bf16[4,2048,128]{2,1,0:T(8,128)(2,1)S(1)}, u32[]{:S(2)}, u32[]{:S(2)}) collective-permute-start(bf16[4,2048,128]{2,1,0:T(8,128)(2,1)S(1)} %collective-permute-done.1), channel_id=1, source_target_pairs={{0,1},{1,2},{2,3},{3,4},{4,5},{5,6},{6,7},{7,0},{8,9},{9,10},{10,1... | collective-permute-start | bytes 6291464 | tf_op jit(solution)/shard_map/ppermute | solution.py:95
  150.9 1.4 copy-start.5
  152.3 67.8 %collective-permute-start.3 = (bf16[4,2048,128]{2,1,0:T(8,128)(2,1)S(1)}, bf16[4,2048,128]{2,1,0:T(8,128)(2,1)S(1)}, u32[]{:S(2)}, u32[]{:S(2)}) collective-permute-start(bf16[4,2048,128]{2,1,0:T(8,128)(2,1)S(1)} %collective-permute-done.2), channel_id=1, source_target_pairs={{0,1},{1,2},{2,3},{3,4},{4,5},{5,6},{6,7},{7,0},{8,9},{9,10},{10,1... | collective-permute-start | bytes 6291464 | tf_op jit(solution)/shard_map/ppermute | solution.py:95
  220.0 1.4 copy-start.7
  221.4 70.4 %collective-permute-start.4 = (bf16[4,2048,128]{2,1,0:T(8,128)(2,1)S(1)}, bf16[4,2048,128]{2,1,0:T(8,128)(2,1)S(1)}, u32[]{:S(2)}, u32[]{:S(2)}) collective-permute-start(bf16[4,2048,128]{2,1,0:T(8,128)(2,1)S(1)} %collective-permute-done.3), channel_id=1, source_target_pairs={{0,1},{1,2},{2,3},{3,4},{4,5},{5,6},{6,7},{7,0},{8,9},{9,10},{10,1... | collective-permute-start | bytes 6291464 | tf_op jit(solution)/shard_map/ppermute | solution.py:95
  291.8 1.3 copy-start.9
  293.1 71.5 %collective-permute-start.5 = (bf16[4,2048,128]{2,1,0:T(8,128)(2,1)S(1)}, bf16[4,2048,128]{2,1,0:T(8,128)(2,1)}, u32[]{:S(2)}, u32[]{:S(2)}) collective-permute-start(bf16[4,2048,128]{2,1,0:T(8,128)(2,1)S(1)} %collective-permute-done.4), channel_id=1, source_target_pairs={{0,1},{1,2},{2,3},{3,4},{4,5},{5,6},{6,7},{7,0},{8,9},{9,10},{10,1... | collective-permute-start | bytes 6291464 | tf_op jit(solution)/shard_map/ppermute | solution.py:95
  364.5 66.6 %collective-permute-start.6 = (bf16[4,2048,128]{2,1,0:T(8,128)(2,1)}, bf16[4,2048,128]{2,1,0:T(8,128)(2,1)}, u32[]{:S(2)}, u32[]{:S(2)}) collective-permute-start(bf16[4,2048,128]{2,1,0:T(8,128)(2,1)} %collective-permute-done.5), channel_id=1, source_target_pairs={{0,1},{1,2},{2,3},{3,4},{4,5},{5,6},{6,7},{7,0},{8,9},{9,10},{10,1... | collective-permute-start | bytes 6291464 | tf_op jit(solution)/shard_map/ppermute | solution.py:95
  376.5 3.9 copy-start.13
  376.5 56.0 %all-to-all-start.1 = ((bf16[16,48,2048]{2,1,0:T(8,128)(2,1)}), bf16[16,48,2048]{2,1,0:T(8,128)(2,1)S(1)}, u32[]{:S(2)}, u32[]{:S(2)}) async-start(bf16[16,48,2048]{2,1,0:T(8,128)(2,1)} %bitcast.7), calls=%async_computation.1 | async-start | bytes 6291456 | tf_op jit(solution)/shard_map/all_to_all | solution.py:87
  380.3 51.1 %copy-start.17 = (f32[128]{0:T(128)S(1)}, f32[128]{0:T(128)}, u32[]{:S(2)}) copy-start(f32[128]{0:T(128)} %param.11) | copy-start | bytes 1540
  380.3 169.3 %all-gather.4.cloned.1.call-start = ((), (), s32[]{:S(2)}) async-start(), calls=%async_computation.3 | async-start | bytes 4718592 | tf_op jit(solution)/shard_map/all_gather | solution.py:73
  380.4 50.8 %collective-permute-start = (bf16[15,128]{1,0:T(8,128)(2,1)S(1)}, bf16[15,128]{1,0:T(8,128)(2,1)S(1)}, u32[]{:S(2)}, u32[]{:S(2)}) collective-permute-start(bf16[15,128]{1,0:T(8,128)(2,1)S(1)} %slice.57), channel_id=1, source_target_pairs={{0,8},{8,16},{16,24},{1,9},{9,17},{17,25},{2,10},{10,18},{18,26},{... | collective-permute-start | bytes 11528 | tf_op jit(solution)/shard_map/ppermute | solution.py:16
  431.1 63.7 %collective-permute-start.7 = (bf16[4,2048,128]{2,1,0:T(8,128)(2,1)}, bf16[4,2048,128]{2,1,0:T(8,128)(2,1)}, u32[]{:S(2)}, u32[]{:S(2)}) collective-permute-start(bf16[4,2048,128]{2,1,0:T(8,128)(2,1)} %collective-permute-done.6), channel_id=1, source_target_pairs={{0,1},{1,2},{2,3},{3,4},{4,5},{5,6},{6,7},{7,0},{8,9},{9,10},{10,1... | collective-permute-start | bytes 6291464 | tf_op jit(solution)/shard_map/ppermute | solution.py:95
  432.5 4.5 copy-start
  432.5 111.5 %all-to-all-start = ((bf16[8,128,128]{2,1,0:T(8,128)(2,1)}), bf16[8,128,128]{2,1,0:T(8,128)(2,1)S(1)}, u32[]{:S(2)}, u32[]{:S(2)}) async-start(bf16[8,128,128]{2,1,0:T(8,128)(2,1)} %bitcast), calls=%async_computation | async-start | bytes 524288 | tf_op jit(solution)/shard_map/all_to_all | solution.py:70
  501.5 3.5 copy-start.10
  505.0 1.8 copy-start.8
  506.8 1.8 copy-start.6
  508.6 1.8 copy-start.4
  510.4 1.9 copy-start.2
  543.9 4.6 copy-start.16
  543.9 0.7 copy-start.12
  544.6 24.5 %all-to-all-start.2 = ((bf16[4,192,2048]{2,0,1:T(4,128)(2,1)}), bf16[4,192,2048]{2,0,1:T(4,128)(2,1)S(1)}, u32[]{:S(2)}, u32[]{:S(2)}) async-start(bf16[4,192,2048]{2,0,1:T(4,128)(2,1)} %copy.52), calls=%async_computation.2 | async-start | bytes 6291456 | tf_op jit(solution)/shard_map/all_to_all | solution.py:107
Sparse Core Ops, SparseCore 0:
  9.6 209.1 all-gather.5
  220.3 209.8 all-gather.7
  431.8 51.0 all-gather.3
